TPU v7x, 32 devices: a whole 2x2x4 slice. The times are simulated.
32 devices in a mesh: grp: 2 (over x), row: 4 (over z), col: 4 (over y, core).
Axes of the slice: x: 2, y: 2, z: 4, core: 2. Of those that a mesh axis runs over, the one named last changes fastest.
Arguments:
- gate_in: bfloat16 [8, 512, 1024], P(('grp', 'row'), 'col'), parts along dimension 0, may hold values from -6 to 6
- mult_in: bfloat16 [8, 512, 1024], P(('grp', 'row'), 'col'), parts along dimension 0, may hold values from -6 to 6
- value_in: bfloat16 [8, 512, 1024], P(('grp', 'row'), 'col'), parts along dimension 0, may hold values from -6 to 6
- taps_gate: float32 [3, 1024], replicated, may hold values from -3.5 to 3.5
- taps_mult: float32 [3, 1024], replicated, may hold values from -3.5 to 3.5
- taps_value: float32 [3, 1024], replicated, may hold values from -3.5 to 3.5
- filter_first: float32 [33, 128], replicated, may hold values from -3 to 3
- filter_second: float32 [128, 128], replicated, may hold values from -1 to 1
- filter_ahead: float32 [128, 1024], replicated, may hold values from -0.5 to 0.5
- filter_behind: float32 [128, 1024], replicated, may hold values from -0.5 to 0.5
- filter_decay: float32 [1024], replicated, may hold values from 0.05 to 17.033333
- skip_gain: float32 [1024], replicated, may hold values from -5 to 5
- out_weight: bfloat16 [1024, 2048], replicated, may hold values from -0.1875 to 0.1875
Outputs:
- mixed: bfloat16 [8, 512, 2048], P(('grp', 'row'), 'col'), parts along dimension 0
There are 2 independent parts, one for each index of `grp`. A program takes and returns all parts, laid end to end along the dimension named above; an argument that names none is the same for every part. Nothing has to cross between parts.
All inputs are finite; a program needn't handle non-finite values.
Results may differ from a plain program's by a relative error of at most 0.0049.
Values may be sent and summed in bfloat16 or wider, within the bound.
A program may use at most 64 MiB of HBM per device.

v0:
```python
import math
import jax
import jax.numpy as jnp
from jax import lax
from jax.sharding import PartitionSpec as P

highest = lax.Precision.HIGHEST


def padded_2(shard, sides, width):
    for axis, dim in sides:
        size, length = (lax.axis_size(axis), shard.shape[dim])
        up = [(i, (i + 1) % size) for i in range(size - 1)]
        down = [(j, i) for i, j in up]
        last = lax.slice_in_dim(shard, length - width, length, axis=dim)
        leading = lax.slice_in_dim(shard, 0, width, axis=dim)
        before = lax.ppermute(last, axis, up)
        after = lax.ppermute(leading, axis, down)
        shard = jnp.concatenate([before, shard, after], axis=dim)
    return shard


def filter_hidden(mirror, seq_len, filter_first, filter_second):
    tau_values = mirror.astype(jnp.float32) / (seq_len - 1)
    omega_pos = 2.0 * math.pi / seq_len * mirror.astype(jnp.float32)
    band_count = (filter_first.shape[0] - 1) // 2
    band_values = jnp.linspace(0.0001, band_count - 1, band_count, dtype=jnp.float32)
    angles = omega_pos[:, None] * band_values[None, :]
    features = jnp.concatenate([tau_values[:, None], jnp.cos(angles), -jnp.sin(angles)], axis=1)
    hidden = jnp.sin(jnp.dot(features, filter_first, precision=highest))
    hidden = jnp.sin(jnp.dot(hidden, filter_second, precision=highest))
    return (hidden, tau_values)


def side_values(hidden, tau_values, side_weight, decay_rates):
    values = jnp.einsum("pf,fh->hp", hidden, side_weight, precision=highest)
    return values * jnp.exp(-decay_rates[:, None] * tau_values[None, :])


def angle_table(row_count, column_count, period):
    products = (
        lax.iota(jnp.int32, row_count)[:, None]
        * lax.iota(jnp.int32, column_count)[None, :]
        % period
    )
    angle = products.astype(jnp.float32) * (2.0 * math.pi / period)
    return (jnp.cos(angle), jnp.sin(angle))


def swap_halves(stacked, width):
    return jnp.concatenate([stacked[..., width:], stacked[..., :width]], axis=-1)


def forward(values, first_table, twist_even, twist_odd, second_block):
    channels, _, width = values.shape
    first = jnp.einsum("sfa,cab->cfsb", first_table, values, precision=highest)
    first = first.reshape(channels, first_table.shape[1], 2 * width)
    turned = first * twist_even + swap_halves(first, width) * twist_odd
    return jnp.einsum("cfk,kl->cfl", turned, second_block, precision=highest)


def inverse(spectrum, last_table, twist_even, twist_odd, second_block, span_len):
    channels, freq_rows, double_width = spectrum.shape
    width = double_width // 2
    back = jnp.einsum("cfk,kl->cfl", spectrum, second_block, precision=highest)
    turned = back * twist_even + swap_halves(back, width) * twist_odd
    turned = turned.reshape(channels, freq_rows, 2, width)
    result = jnp.einsum("asf,cfsb->cab", last_table, turned, precision=highest)
    return result / span_len


def body(
    gate_in,
    mult_in,
    value_in,
    taps_gate,
    taps_mult,
    taps_value,
    filter_first,
    filter_second,
    filter_ahead,
    filter_behind,
    filter_decay,
    skip_gain,
    out_weight,
):
    col_count = lax.axis_size("col")
    col_index = lax.axis_index("col")
    tok_rows = gate_in.shape[1]
    seq_len = tok_rows * col_count
    span_len = 2 * seq_len
    group_size = filter_ahead.shape[1] // col_count
    stacked = jnp.stack([gate_in[0], mult_in[0], value_in[0]])
    padded = padded_2(stacked, (("col", 1),), 1).astype(jnp.float32)
    all_taps = jnp.stack([taps_gate, taps_mult, taps_value])
    shorted = jnp.zeros(stacked.shape, jnp.float32)
    for offset in range(all_taps.shape[1]):
        shorted = shorted + all_taps[:, offset][:, None, :] * padded[:, offset : offset + tok_rows]
    gate_part = shorted[0]
    product = shorted[2] * shorted[1]
    spread = lax.all_to_all(product.T, "col", split_axis=0, concat_axis=1, tiled=True)
    first_channel = col_index * group_size
    own_rates = lax.dynamic_slice_in_dim(filter_decay, first_channel, group_size)
    mirror = lax.iota(jnp.int32, seq_len)
    hidden, tau_values = filter_hidden(mirror, seq_len, filter_first, filter_second)
    ahead_vals = side_values(
        hidden,
        tau_values,
        lax.dynamic_slice_in_dim(filter_ahead, first_channel, group_size, 1),
        own_rates,
    )
    behind_vals = side_values(
        hidden,
        tau_values,
        lax.dynamic_slice_in_dim(filter_behind, first_channel, group_size, 1),
        own_rates,
    )
    kernel = jnp.concatenate(
        [ahead_vals, jnp.zeros((group_size, 1), jnp.float32), jnp.flip(behind_vals[:, 1:], axis=1)],
        axis=1,
    )
    kernel = kernel * lax.rsqrt(jnp.sum(kernel * kernel, axis=1, keepdims=True) + 1e-06)
    factor = 128
    half_rows = factor // 2
    width_second = span_len // factor
    first_cos, first_sin = angle_table(factor, factor, factor)
    twist_cos, twist_sin = angle_table(factor, width_second, span_len)
    second_cos, second_sin = angle_table(width_second, width_second, width_second)
    first_table = jnp.stack([first_cos, -first_sin])
    last_table = jnp.stack([first_cos[:half_rows], -first_sin[:half_rows]], axis=1)
    twist_even = jnp.concatenate([twist_cos, twist_cos], axis=1)
    twist_ahead = jnp.concatenate([twist_sin, -twist_sin], axis=1)
    twist_back = jnp.concatenate([-twist_sin, twist_sin], axis=1)
    block_ahead = jnp.concatenate(
        [
            jnp.concatenate([second_cos, -second_sin], axis=1),
            jnp.concatenate([second_sin, second_cos], axis=1),
        ],
        axis=0,
    )
    block_back = jnp.concatenate(
        [
            jnp.concatenate([second_cos, second_sin], axis=1),
            jnp.concatenate([-second_sin, second_cos], axis=1),
        ],
        axis=0,
    )
    kernel_spec = forward(
        kernel.reshape(group_size, factor, width_second),
        first_table,
        twist_even,
        twist_ahead,
        block_ahead,
    )
    data_spec = forward(
        spread.reshape(group_size, half_rows, width_second),
        first_table[:, :, :half_rows],
        twist_even,
        twist_ahead,
        block_ahead,
    )
    data_re = data_spec[..., :width_second]
    data_im = data_spec[..., width_second:]
    kernel_re = kernel_spec[..., :width_second]
    kernel_im = kernel_spec[..., width_second:]
    joined = jnp.concatenate(
        [data_re * kernel_re - data_im * kernel_im, data_re * kernel_im + data_im * kernel_re],
        axis=-1,
    )
    convolved = inverse(joined, last_table, twist_even, twist_back, block_back, span_len).reshape(
        group_size, seq_len
    )
    returned = lax.all_to_all(convolved, "col", split_axis=1, concat_axis=0, tiled=True)
    mixed_rows = ((returned.T + skip_gain * product) * gate_part).astype(jnp.bfloat16)
    return jnp.dot(mixed_rows, out_weight, preferred_element_type=jnp.float32).astype(jnp.bfloat16)[
        None
    ]


def solution(mesh):
    in_specs = (
        P(("grp", "row"), "col", None),
        P(("grp", "row"), "col", None),
        P(("grp", "row"), "col", None),
        P(),
        P(),
        P(),
        P(),
        P(),
        P(),
        P(),
        P(),
        P(),
        P(),
    )
    out_specs = P(("grp", "row"), "col", None)
    return jax.shard_map(body, mesh=mesh, in_specs=in_specs, out_specs=out_specs, check_vma=False)
```

profile of v0, /device:TPU:0, one launch (start us, length us, event | category | flops | bytes accessed | tf_op | source)
XLA Modules:
  0.0 80.0 jit_solution(17331171744776615139)
XLA Ops:
  0.0 1.2 %copy.37 = bf16[1,128,1024]{1,2,0:T(8,128)(2,1)S(1)} copy(bf16[1,128,1024]{2,1,0:T(8,128)(2,1)} %param.13) | data formatting | bytes 524288 | tf_op args[0]
  1.2 1.2 %copy.38 = bf16[1,128,1024]{1,2,0:T(8,128)(2,1)S(1)} copy(bf16[1,128,1024]{2,1,0:T(8,128)(2,1)} %param.14) | data formatting | bytes 524288 | tf_op args[1]
  2.4 1.2 %copy.39 = bf16[1,128,1024]{1,2,0:T(8,128)(2,1)S(1)} copy(bf16[1,128,1024]{2,1,0:T(8,128)(2,1)} %param.15) | data formatting | bytes 524288 | tf_op args[2]
  3.7 0.7 copy-done.6
  4.4 0.1 pad_maximum_fusion.1
  4.5 0.0 copy-start.16
  4.5 0.3 fusion.116
  4.8 0.4 copy.40
  5.2 3.0 %collective-permute-start = (bf16[3,1,1024]{2,0,1:T(4,128)(2,1)S(1)}, bf16[3,1,1024]{2,0,1:T(4,128)(2,1)}, u32[]{:S(2)}, u32[]{:S(2)}) collective-permute-start(bf16[3,1,1024]{2,0,1:T(4,128)(2,1)S(1)} %copy.40), channel_id=1, source_target_pairs={{0,1},{1,2},{2,3},{4,5},{5,6},{6,7},{8,9},{9,10},{10,11},{12,13},{... | collective-permute-start | bytes 18440 | tf_op jit(solution)/shard_map/ppermute | solution.py:17
  8.1 1.0 %copy.41 = bf16[3,1,1024]{2,0,1:T(4,128)(2,1)} copy(bf16[3,1,1024]{1,2,0:T(8,128)(2,1)S(1)} %get-tuple-element.16) | data formatting | bytes 12288 | tf_op jit(solution)/shard_map/slice | solution.py:16
  9.1 1.3 %collective-permute-start.1 = (bf16[3,1,1024]{2,0,1:T(4,128)(2,1)}, bf16[3,1,1024]{2,0,1:T(4,128)(2,1)}, u32[]{:S(2)}, u32[]{:S(2)}) collective-permute-start(bf16[3,1,1024]{2,0,1:T(4,128)(2,1)} %copy.41), channel_id=1, source_target_pairs={{1,0},{2,1},{3,2},{5,4},{6,5},{7,6},{9,8},{10,9},{11,10},{13,12},{... | collective-permute-start | bytes 18440 | tf_op jit(solution)/shard_map/ppermute | solution.py:18
  10.5 0.3 sine_negate_fusion
  10.7 0.1 fusion.98
  10.8 0.7 fusion.96
  11.5 0.1 fusion.99
  11.6 0.1 pad_maximum_fusion.15
  11.6 0.2 multiply_cosine_fusion
  11.8 1.3 %convolution_sine_fusion.1 = f32[512,128]{1,0:T(8,128)S(1)} fusion(f32[33,128]{1,0:T(8,128)S(1)} %copy-done.16, f32[512,16]{0,1:T(8,128)S(1)} %get-tuple-element.25, f32[512,16]{0,1:T(8,128)S(1)} %get-tuple-element.24, f32[512,1]{0,1:T(1,128)S(1)} %convert_multiply_fusion.2), kind=kOutput, calls=%fused_computation.40 | convolution fusion | flops 25986048 | bytes 346624 | tf_op jit(solution)/shard_map/dot_general | solution.py:30
  13.2 1.2 %convolution_sine_fusion = f32[512,128]{1,0:T(8,128)S(1)} fusion(f32[512,128]{1,0:T(8,128)S(1)} %convolution_sine_fusion.1, f32[128,128]{1,0:T(8,128)S(1)} %copy-done.12), kind=kOutput, calls=%fused_computation.39 | convolution fusion | flops 100663296 | bytes 589824 | tf_op jit(solution)/shard_map/dot_general | solution.py:31
  14.4 0.8 dynamic-slice_negate_fusion
  15.1 0.6 fusion.48
  15.8 0.1 multiply_exponential_fusion
  15.9 0.3 slice_multiply_fusion.3
  16.3 0.8 reverse
  17.0 0.2 slice.164
  17.2 1.6 %convolution_multiply_fusion = f32[256,512]{1,0:T(8,128)S(1)} fusion(f32[512,128]{1,0:T(8,128)S(1)} %convolution_sine_fusion, f32[512]{0:T(512)S(1)} %convert_multiply_fusion, f32[256]{0:T(256)S(1)} %dynamic-slice_negate_fusion, f32[128,1024]{1,0:T(8,128)} %param.21, s32[]{:T(128)S(6)} %select_n.68), kind=kOutput, calls=%fused_computation.38 | convolution fusion | flops 201588736 | bytes 920580 | tf_op jit(solution)/shard_map/pf,fh->hp/dot_general | solution.py:36
  18.8 0.3 multiply_reduce_fusion
  19.1 0.3 copy.47
  19.5 0.1 fusion.36
  19.5 1.8 %convolution_bitcast_fusion = f32[256,128,2,8]{1,0,2,3:T(8,128)S(1)} fusion(f32[256,128,8,1]{0,2,1,3:T(8,128)S(1)} %fusion.36, f32[1,128,128]{1,2,0:T(8,128)S(1)} %get-tuple-element.28, f32[1,128,128]{1,2,0:T(8,128)S(1)} %get-tuple-element.29), kind=kOutput, calls=%fused_computation.27 | convolution fusion | flops 805339136 | bytes 3276800 | tf_op jit(solution)/shard_map/sfa,cab->cfsb/dot_general | solution.py:56
  21.4 1.2 %copy.80 = f32[256,128,2,8]{1,3,2,0:T(8,128)S(1)} copy(f32[256,128,2,8]{1,0,2,3:T(8,128)S(1)} %convolution_bitcast_fusion) | data formatting | bytes 4194304 | tf_op jit(solution)/shard_map/sfa,cab->cfsb/transpose | solution.py:56
  22.6 0.0 copy-start.18
  22.7 0.0 copy-start.19
  22.7 1.5 %fusion.115 = (f32[256,128,8]{1,2,0:T(8,128)}, f32[256,128,8]{1,2,0:T(8,128)}) fusion(f32[256,128,16]{1,2,0:T(8,128)S(1)} %bitcast.107), kind=kLoop, calls=%fused_computation.171 | loop fusion | bytes 4194304 | tf_op jit(solution)/shard_map/slice | solution.py:51
  24.1 0.8 cosine_bitcast_fusion
  24.9 0.6 pad_maximum_fusion.14
  25.5 0.6 copy_bitcast_fusion.2
  26.2 0.6 copy.82
  26.8 1.1 %copy.42 = bf16[3,1,1024]{1,2,0:T(8,128)(2,1)S(1)} copy(bf16[3,1,1024]{2,0,1:T(4,128)(2,1)} %collective-permute-done) | data formatting | bytes 12288 | tf_op jit(solution)/shard_map/ppermute | solution.py:17
  27.9 1.9 %copy.43 = bf16[3,1,1024]{1,2,0:T(8,128)(2,1)} copy(bf16[3,1,1024]{2,0,1:T(4,128)(2,1)} %collective-permute-done.1) | data formatting | bytes 12288 | tf_op jit(solution)/shard_map/ppermute | solution.py:18
  29.8 2.2 %maximum_convert_fusion = f32[3,130,1024]{1,2,0:T(8,128)S(1)} fusion(bf16[3,1,1024]{1,2,0:T(8,128)(2,1)} %copy.43, bf16[1,128,1024]{1,2,0:T(8,128)(2,1)} %copy-done.6, bf16[1,128,1024]{1,2,0:T(8,128)(2,1)} %copy-done.5, bf16[1,128,1024]{1,2,0:T(8,128)(2,1)} %copy-done.4, bf16[3,1,1024]{1,2,0:T(8,128)(2,1)S(1)} %copy.42), kind=kLoop, calls=%fused_computation.34 | loop fusion | flops 3993600 | bytes 2396160 | tf_op jit(solution)/shard_map/convert_element_type | solution.py:94
  32.1 2.3 %fusion.24 = f32[3,128,1024]{1,2,0:T(8,128)S(1)} fusion(f32[3,130,1024]{1,2,0:T(8,128)S(1)} %maximum_convert_fusion, f32[3,1024]{1,0:T(4,128)S(1)} %copy-done.9, f32[3,1024]{1,0:T(4,128)S(1)} %copy-done.10, f32[3,1024]{1,0:T(4,128)S(1)} %bitcast.114), kind=kLoop, calls=%fused_computation.30 | loop fusion | flops 1966080 | bytes 6328320 | tf_op jit(solution)/shard_map/add | solution.py:98
  34.4 1.1 %copy-done.1 = f32[3,128,1024]{1,2,0:T(8,128)} copy-done((f32[3,128,1024]{1,2,0:T(8,128)}, f32[3,128,1024]{1,2,0:T(8,128)S(1)}, u32[]{:S(2)}) %copy-start.1) | copy-done | bytes 1572888
  35.6 0.8 %slice_multiply_fusion.4 = f32[1,128,1024]{1,2,0:T(8,128)} fusion(f32[3,128,1024]{1,2,0:T(8,128)S(1)} %fusion.24), kind=kLoop, calls=%fused_computation.59 | loop fusion | flops 131072 | bytes 1572864 | tf_op jit(solution)/shard_map/mul | solution.py:100
  36.4 5.6 %all-to-all-start = ((f32[4,256,128]{2,1,0:T(8,128)}), f32[4,256,128]{2,1,0:T(8,128)S(1)}, u32[]{:S(2)}, u32[]{:S(2)}) async-start(f32[4,256,128]{2,1,0:T(8,128)} %bitcast.5), calls=%async_computation | async-start | bytes 1048576 | tf_op jit(solution)/shard_map/all_to_all | solution.py:101
  42.0 0.1 fusion.101
  42.0 6.1 %fusion.7 = f32[256,128,16]{1,2,0:T(8,128)} fusion(f32[256,128,8]{1,2,0:T(8,128)} %get-tuple-element.14, f32[256,128,8]{1,2,0:T(8,128)} %get-tuple-element.13, f32[128,16]{0,1:T(8,128)S(1)} %get-tuple-element.23, f32[128,16]{0,1:T(8,128)S(1)} %pad_maximum_fusion.12, f32[8,8]{0,1:T(8,128)S(1)} %copy-done.14, f32[8,8]{0,1:T(8,128)S(1)} %copy-done.13, ...), kind=kOutput, calls=%fused_computation.9 | convolution fusion | flops 102761216 | bytes 6308608 | tf_op jit(solution)/shard_map/cfk,kl->cfl/dot_general | solution.py:59
  48.1 2.7 %all-to-all-done = f32[4,256,128]{2,1,0:T(8,128)S(1)} async-done(((f32[4,256,128]{2,1,0:T(8,128)}), f32[4,256,128]{2,1,0:T(8,128)S(1)}, u32[]{:S(2)}, u32[]{:S(2)}) %all-to-all-start) | async-done | bytes 524320 | tf_op jit(solution)/shard_map/all_to_all | solution.py:101
  50.8 0.2 copy.44
  51.0 1.9 %convolution_bitcast_fusion.1 = f32[256,128,2,8]{1,0,2,3:T(8,128)S(1)} fusion(f32[256,64,8,1]{0,2,1,3:T(8,128)S(1)} %bitcast.113, f32[1,128,128]{1,2,0:T(8,128)S(1)} %get-tuple-element.29, f32[1,128,128]{1,2,0:T(8,128)S(1)} %get-tuple-element.28), kind=kOutput, calls=%fused_computation.28 | convolution fusion | flops 402669568 | bytes 2752512 | tf_op jit(solution)/shard_map/sfa,cab->cfsb/dot_general | solution.py:56
  52.9 1.2 %copy.81 = f32[256,128,2,8]{1,3,2,0:T(8,128)S(1)} copy(f32[256,128,2,8]{1,0,2,3:T(8,128)S(1)} %convolution_bitcast_fusion.1) | data formatting | bytes 4194304 | tf_op jit(solution)/shard_map/sfa,cab->cfsb/transpose | solution.py:56
  54.1 0.1 fusion.114
  54.2 3.1 %fusion.2 = f32[256,128,16]{1,2,0:T(8,128)S(1)} fusion(f32[256,128,8]{1,2,0:T(8,128)S(1)} %get-tuple-element.12, f32[256,128,8]{1,2,0:T(8,128)S(1)} %get-tuple-element.11, f32[128,16]{0,1:T(8,128)S(1)} %get-tuple-element.23, f32[128,16]{0,1:T(8,128)S(1)} %pad_maximum_fusion.12, f32[8,8]{0,1:T(8,128)S(1)} %copy-done.14, f32[8,8]{0,1:T(8,128)S(1)} %copy-done.13, ...), kind=kOutput, calls=%fused_computation.4 | convolution fusion | flops 102761216 | bytes 6308608 | tf_op jit(solution)/shard_map/cfk,kl->cfl/dot_general | solution.py:59
  57.4 0.2 multiply_subtract_fusion
  57.6 2.1 %fusion.11 = f32[256,128,16]{1,2,0:T(8,128)S(1)} fusion(f32[256,128,8]{1,2,0:T(8,128)S(1)} %get-tuple-element.8, f32[256,128,8]{1,2,0:T(8,128)S(1)} %get-tuple-element.7, f32[8,8]{0,1:T(8,128)S(1)} %copy-done.14, f32[8,8]{0,1:T(8,128)S(1)} %fusion.101, f32[8,8]{0,1:T(8,128)S(1)} %copy-done.13), kind=kOutput, calls=%fused_computation.12 | convolution fusion | flops 101188352 | bytes 4195072 | tf_op jit(solution)/shard_map/cfk,kl->cfl/dot_general | solution.py:65
  59.8 0.1 fusion.113
  59.9 0.6 copy-done.7
  60.5 0.0 copy-done.8
  60.5 1.8 %fusion.32 = f32[256,64,8]{1,2,0:T(8,128)S(1)} fusion(f32[256,128,8]{1,2,0:T(8,128)S(1)} %get-tuple-element.10, f32[256,128,8]{1,2,0:T(8,128)S(1)} %get-tuple-element.9, f32[256,128,16]{1,2,0:T(8,128)S(1)} %fusion.11, f32[128,16]{0,1:T(8,128)S(1)} %copy-done.15, f32[128,16]{0,1:T(8,128)S(1)} %pad_maximum_fusion.12, f32[64,1,128]{2,0,1:T(8,128)S(1)} %copy-done.8, ...), kind=kOutput, calls=%fused_computation.37 | convolution fusion | flops 404897792 | bytes 4800512 | tf_op jit(solution)/shard_map/asf,cfsb->cab/dot_general | solution.py:68
  62.4 1.2 %copy.51 = f32[256,64,8]{0,2,1:T(8,128)} copy(f32[256,64,8]{1,2,0:T(8,128)S(1)} %fusion.32) | data formatting | bytes 1048576 | tf_op jit(solution)/shard_map/div | solution.py:69
  63.6 12.3 %all_to_all.35 = f32[256,4,128]{0,2,1:T(8,128)S(1)} all-to-all(f32[256,4,128]{0,2,1:T(8,128)} %bitcast.110), channel_id=1, replica_groups=mesh['grp'=2,'row'=4,'col'=4] {'col'}, dimensions={1} | all-to-all | bytes 1048576 | tf_op jit(solution)/shard_map/all_to_all | solution.py:173
  75.8 0.2 copy.52
  76.1 0.2 fusion.44
  76.3 3.7 %fusion = bf16[1,128,2048]{2,1,0:T(8,128)(2,1)} fusion(bf16[128,1024]{0,1:T(8,128)(2,1)S(1)} %fusion.44, bf16[1024,2048]{1,0:T(8,128)(2,1)} %param.25), kind=kOutput, calls=%fused_computation.1 | convolution fusion | flops 537133056 | bytes 4980736 | tf_op jit(solution)/shard_map/dot_general | solution.py:175
  (46 shorter events, 0.2 us)
Async XLA Ops:
  0.0 15.1 %copy-start = (f32[128,1024]{1,0:T(8,128)S(1)}, f32[128,1024]{1,0:T(8,128)}, u32[]{:S(2)}) copy-start(f32[128,1024]{1,0:T(8,128)} %param.22) | copy-start | bytes 1572868
  1.2 2.5 %copy-start.4 = (bf16[1,128,1024]{1,2,0:T(8,128)(2,1)}, bf16[1,128,1024]{1,2,0:T(8,128)(2,1)S(1)}, u32[]{:S(2)}) copy-start(bf16[1,128,1024]{1,2,0:T(8,128)(2,1)S(1)} %copy.37) | copy-start | bytes 786436
  2.4 1.2 %copy-start.5 = (bf16[1,128,1024]{1,2,0:T(8,128)(2,1)}, bf16[1,128,1024]{1,2,0:T(8,128)(2,1)S(1)}, u32[]{:S(2)}) copy-start(bf16[1,128,1024]{1,2,0:T(8,128)(2,1)S(1)} %copy.38) | copy-start | bytes 786436
  3.7 0.7 copy-start.6
  4.5 7.4 %copy-start.16 = (f32[33,128]{1,0:T(8,128)S(1)}, f32[33,128]{1,0:T(8,128)}, u32[]{:S(2)}) copy-start(f32[33,128]{1,0:T(8,128)} %param.19) | copy-start | bytes 50692
  4.5 8.7 %copy-start.12 = (f32[128,128]{1,0:T(8,128)S(1)}, f32[128,128]{1,0:T(8,128)}, u32[]{:S(2)}) copy-start(f32[128,128]{1,0:T(8,128)} %param.20) | copy-start | bytes 196612
  5.2 21.6 %collective-permute-start = (bf16[3,1,1024]{2,0,1:T(4,128)(2,1)S(1)}, bf16[3,1,1024]{2,0,1:T(4,128)(2,1)}, u32[]{:S(2)}, u32[]{:S(2)}) collective-permute-start(bf16[3,1,1024]{2,0,1:T(4,128)(2,1)S(1)} %copy.40), channel_id=1, source_target_pairs={{0,1},{1,2},{2,3},{4,5},{5,6},{6,7},{8,9},{9,10},{10,11},{12,13},{... | collective-permute-start | bytes 18440 | tf_op jit(solution)/shard_map/ppermute | solution.py:17
  9.1 18.8 %collective-permute-start.1 = (bf16[3,1,1024]{2,0,1:T(4,128)(2,1)}, bf16[3,1,1024]{2,0,1:T(4,128)(2,1)}, u32[]{:S(2)}, u32[]{:S(2)}) collective-permute-start(bf16[3,1,1024]{2,0,1:T(4,128)(2,1)} %copy.41), channel_id=1, source_target_pairs={{1,0},{2,1},{3,2},{5,4},{6,5},{7,6},{9,8},{10,9},{11,10},{13,12},{... | collective-permute-start | bytes 18440 | tf_op jit(solution)/shard_map/ppermute | solution.py:18
  22.6 2.9 %copy-start.17 = (f32[3,1024]{1,0:T(4,128)S(1)}, f32[3,1024]{1,0:T(4,128)}, u32[]{:S(2)}) copy-start(f32[3,1024]{1,0:T(4,128)} %param.18) | copy-start | bytes 36868
  22.6 2.8 %copy-start.18 = (f32[3,1024]{1,0:T(4,128)S(1)}, f32[3,1024]{1,0:T(4,128)}, u32[]{:S(2)}) copy-start(f32[3,1024]{1,0:T(4,128)} %param.17) | copy-start | bytes 36868
  22.7 2.8 %copy-start.19 = (f32[3,1024]{1,0:T(4,128)S(1)}, f32[3,1024]{1,0:T(4,128)}, u32[]{:S(2)}) copy-start(f32[3,1024]{1,0:T(4,128)} %param.16) | copy-start | bytes 36868
  29.8 2.2 %copy-start.9 = (f32[3,1024]{1,0:T(4,128)S(1)}, f32[3,1024]{1,0:T(4,128)}, u32[]{:S(2)}) copy-start(f32[3,1024]{1,0:T(4,128)} %get-tuple-element.26) | copy-start | bytes 36868
  29.8 2.2 %copy-start.10 = (f32[3,1024]{1,0:T(4,128)S(1)}, f32[3,1024]{1,0:T(4,128)}, u32[]{:S(2)}) copy-start(f32[3,1024]{1,0:T(4,128)} %get-tuple-element.27) | copy-start | bytes 36868
  29.8 2.2 %copy-start.11 = (f32[3,1,1024]{2,0,1:T(4,128)S(1)}, f32[3,1,1024]{2,0,1:T(4,128)}, u32[]{:S(2)}) copy-start(f32[3,1,1024]{2,0,1:T(4,128)} %copy.82) | copy-start | bytes 36868
  34.4 1.1 %copy-start.1 = (f32[3,128,1024]{1,2,0:T(8,128)}, f32[3,128,1024]{1,2,0:T(8,128)S(1)}, u32[]{:S(2)}) copy-start(f32[3,128,1024]{1,2,0:T(8,128)S(1)} %fusion.24) | copy-start | bytes 4718596
  35.6 6.5 %copy-start.13 = (f32[8,8]{0,1:T(8,128)S(1)}, f32[8,8]{0,1:T(8,128)}, u32[]{:S(2)}) copy-start(f32[8,8]{0,1:T(8,128)} %get-tuple-element.32) | copy-start | bytes 772
  35.6 6.5 %copy-start.14 = (f32[8,8]{0,1:T(8,128)S(1)}, f32[8,8]{0,1:T(8,128)}, u32[]{:S(2)}) copy-start(f32[8,8]{0,1:T(8,128)} %get-tuple-element.33) | copy-start | bytes 772
  36.4 14.4 %all-to-all-start = ((f32[4,256,128]{2,1,0:T(8,128)}), f32[4,256,128]{2,1,0:T(8,128)S(1)}, u32[]{:S(2)}, u32[]{:S(2)}) async-start(f32[4,256,128]{2,1,0:T(8,128)} %bitcast.5), calls=%async_computation | async-start | bytes 1048576 | tf_op jit(solution)/shard_map/all_to_all | solution.py:101
  54.2 3.1 %copy-start.3 = (f32[256,128,16]{1,2,0:T(8,128)S(1)}, f32[256,128,16]{1,2,0:T(8,128)}, u32[]{:S(2)}) copy-start(f32[256,128,16]{1,2,0:T(8,128)} %fusion.7) | copy-start | bytes 6291460
  59.8 0.8 copy-start.7
  59.8 0.8 copy-start.8
  59.8 0.8 copy-start.15
  62.4 13.7 %copy-start.2 = (f32[3,128,1024]{1,2,0:T(8,128)S(1)}, f32[3,128,1024]{1,2,0:T(8,128)}, u32[]{:S(2)}) copy-start(f32[3,128,1024]{1,2,0:T(8,128)} %copy-done.1) | copy-start | bytes 4718596
  62.4 13.7 %copy-start.20 = (f32[1024]{0:T(1024)S(1)}, f32[1024]{0:T(1024)}, u32[]{:S(2)}) copy-start(f32[1024]{0:T(1024)} %param.24) | copy-start | bytes 12292
where the time goes:
time: 80.6 us; the launch traced here: 80 us
  matrix products  25.3 us (31%)
  local copies, waits for them, and re-layouts  19.1 us (24%)
  blocking collectives  12.3 us (15%)
  other arithmetic  10.3 us (13%)
  starting transfers between devices  9.83 us (12%)
  waiting for transfers between devices  2.68 us (3%)
    all_to_all x1, blocking collectives, body(): lax.all_to_all(convolved, 'col', split_axis=1, concat_axis=0, tiled=True)  12.3 us
    dot_general x2, matrix products, forward(): return jnp.einsum('cfk,kl->cfl', turned, second_block, precision=highest)  9.19 us
    unnamed x49, local copies, waits for them, and re-layouts  8.32 us
    all_to_all x1, starting transfers between devices, body(): lax.all_to_all(product.T, 'col', split_axis=0, concat_axis=1, tiled=True)  5.57 us
    dot_general x1, matrix products, body(): jnp.dot(mixed_rows, out_weight, preferred_element_type=jnp.float32)  3.73 us
    dot_general x2, matrix products, forward(): first = jnp.einsum('sfa,cab->cfsb', first_table, values, precision=highest)  3.72 us
    ppermute x1, starting transfers between devices, padded_2(): before = lax.ppermute(last, axis, up)  2.98 us
    all_to_all x1, waiting for transfers between devices, body(): lax.all_to_all(product.T, 'col', split_axis=0, concat_axis=1, tiled=True)  2.68 us
  transfers between devices with their start and end apart: 3, of which 1 were waited for; matrix products, arithmetic and copies ran while one was open for 30% of the time, Pallas kernels for 0%

commit v1 on v0

--- a/solution.py
+++ b/solution.py
@@ -98,7 +98,10 @@
         shorted = shorted + all_taps[:, offset][:, None, :] * padded[:, offset : offset + tok_rows]
     gate_part = shorted[0]
     product = shorted[2] * shorted[1]
-    spread = lax.all_to_all(product.T, "col", split_axis=0, concat_axis=1, tiled=True)
+    spread = jnp.concatenate(
+        lax.all_to_all(jnp.stack(jnp.split(product.T, lax.axis_size("col"), axis=0)), "col", 0, 0),
+        axis=1,
+    )
     first_channel = col_index * group_size
     own_rates = lax.dynamic_slice_in_dim(filter_decay, first_channel, group_size)
     mirror = lax.iota(jnp.int32, seq_len)

time: 80.6 us -> 70.7 us (0.88)
  local copies, waits for them, and re-layouts: 19.1 us -> 11.4 us
  other arithmetic: 10.3 us -> 8.18 us
  blocking collectives: 12.3 us -> 11.2 us
  matrix products: 25.3 us -> 26.4 us
    unnamed x49 -> x36, local copies, waits for them, and re-layouts: 8.32 us -> 4.56 us
    ppermute x2 -> x0, local copies, waits for them, and re-layouts: 3.04 us -> none  [the longest x1 1.93 us: padded_2(): after = lax.ppermute(leading, axis, down)]
    add x1, other arithmetic: 2.33 us -> 0.46 us  [body(): shorted + all_taps[:, offset][:, None, :] * padded[:, offset:offset + tok...]
    convert_element_type x1, other arithmetic: 2.22 us -> 0.97 us  [body(): padded = padded_2(stacked, (('col', 1),), 1).astype(jnp.float32)]
    all_to_all x1, blocking collectives: 12.3 us -> 11.2 us  [body(): lax.all_to_all(convolved, 'col', split_axis=1, concat_axis=0, tiled=True)]
    another operation x0 -> x2, local copies, waits for them, and re-layouts: none -> 1.01 us  [the longest x1 0.97 us: body(): stacked = jnp.stack([gate_in[0], mult_in[0], value_in[0]])]
    slice x1 -> x0, local copies, waits for them, and re-layouts: 0.98 us -> none  [padded_2(): leading = lax.slice_in_dim(shard, 0, width, axis=dim)]
    mul x1 -> x0, other arithmetic: 0.85 us -> none  [body(): product = shorted[2] * shorted[1]]
  transfers between devices with their start and end apart: 3 -> 3, of which waited for: 1 -> 1; matrix products, arithmetic and copies ran while one was open for 30% -> 33% of each run, Pallas kernels for 0% -> 0%
where the time goes in v1:
time: 70.7 us; the launch traced here: 70.1 us
  matrix products  26.4 us (37%)
  local copies, waits for them, and re-layouts  11.4 us (16%)
  blocking collectives  11.2 us (16%)
  starting transfers between devices  9.83 us (14%)
  other arithmetic  8.18 us (12%)
  waiting for transfers between devices  2.68 us (4%)
    all_to_all x1, blocking collectives, body(): lax.all_to_all(convolved, 'col', split_axis=1, concat_axis=0, tiled=True)  11.2 us
    dot_general x2, matrix products, forward(): return jnp.einsum('cfk,kl->cfl', turned, second_block, precision=highest)  9.23 us
    all_to_all x1, starting transfers between devices, body(): lax.all_to_all(jnp.stack(jnp.split(product.T, lax.axis_size('col'), axis=...  5.57 us
    unnamed x36, local copies, waits for them, and re-layouts  4.56 us
    dot_general x1, matrix products, body(): jnp.dot(mixed_rows, out_weight, preferred_element_type=jnp.float32)  4.3 us
    dot_general x2, matrix products, forward(): first = jnp.einsum('sfa,cab->cfsb', first_table, values, precision=highest)  3.72 us
    ppermute x1, starting transfers between devices, padded_2(): before = lax.ppermute(last, axis, up)  2.98 us
    all_to_all x1, waiting for transfers between devices, body(): lax.all_to_all(jnp.stack(jnp.split(product.T, lax.axis_size('col'), axis=...  2.67 us
  transfers between devices with their start and end apart: 3, of which 1 were waited for; matrix products, arithmetic and copies ran while one was open for 33% of the time, Pallas kernels for 0%

profile of v1, /device:TPU:0, one launch (start us, length us, event | category | flops | bytes accessed | tf_op | source)
XLA Modules:
  0.0 70.1 jit_solution(16607664024362425979)
XLA Ops:
  0.0 0.0 copy-start
  0.0 1.0 %constant_dynamic-update-slice_fusion.2 = bf16[3,128,1024]{2,1,0:T(8,128)(2,1)S(1)} fusion(bf16[1,128,1024]{2,1,0:T(8,128)(2,1)} %param.13), kind=kLoop, calls=%fused_computation.129 | loop fusion | bytes 524288
  1.0 1.0 %constant_dynamic-update-slice_fusion.1 = bf16[3,128,1024]{2,1,0:T(8,128)(2,1)S(1)} fusion(bf16[3,128,1024]{2,1,0:T(8,128)(2,1)S(1)} %constant_dynamic-update-slice_fusion.2, bf16[1,128,1024]{2,1,0:T(8,128)(2,1)} %param.14), kind=kLoop, calls=%fused_computation.128 | loop fusion | bytes 524288
  2.0 1.0 %constant_dynamic-update-slice_fusion = bf16[3,128,1024]{2,1,0:T(8,128)(2,1)S(1)} fusion(bf16[3,128,1024]{2,1,0:T(8,128)(2,1)S(1)} %constant_dynamic-update-slice_fusion.1, bf16[1,128,1024]{2,1,0:T(8,128)(2,1)} %param.15), kind=kLoop, calls=%fused_computation.127 | loop fusion | bytes 524288 | tf_op jit(solution)/shard_map/stack | solution.py:93
  3.0 0.6 fusion.119
  3.6 3.0 %collective-permute-start = (bf16[3,1,1024]{2,1,0:T(2,128)(2,1)}, bf16[3,1,1024]{2,1,0:T(2,128)(2,1)}, u32[]{:S(2)}, u32[]{:S(2)}) collective-permute-start(bf16[3,1,1024]{2,1,0:T(2,128)(2,1)} %get-tuple-element.15), channel_id=1, source_target_pairs={{0,1},{1,2},{2,3},{4,5},{5,6},{6,7},{8,9},{9,10},{10,11},{12,13},{... | collective-permute-start | bytes 18440 | tf_op jit(solution)/shard_map/ppermute | solution.py:17
  6.6 1.3 %collective-permute-start.1 = (bf16[3,1,1024]{2,1,0:T(2,128)(2,1)}, bf16[3,1,1024]{2,1,0:T(2,128)(2,1)}, u32[]{:S(2)}, u32[]{:S(2)}) collective-permute-start(bf16[3,1,1024]{2,1,0:T(2,128)(2,1)} %get-tuple-element.16), channel_id=1, source_target_pairs={{1,0},{2,1},{3,2},{5,4},{6,5},{7,6},{9,8},{10,9},{11,10},{13,12},{... | collective-permute-start | bytes 18440 | tf_op jit(solution)/shard_map/ppermute | solution.py:18
  7.9 0.3 sine_negate_fusion
  8.2 0.1 fusion.101
  8.2 0.7 fusion.99
  8.9 0.6 fusion.102
  9.5 0.7 fusion.64
  10.2 0.1 pad_maximum_fusion.15
  10.3 0.2 multiply_cosine_fusion
  10.5 2.1 %convolution_sine_fusion.1 = f32[512,128]{1,0:T(8,128)S(1)} fusion(f32[33,128]{1,0:T(8,128)} %param.19, f32[512,16]{0,1:T(8,128)S(1)} %get-tuple-element.29, f32[512,16]{0,1:T(8,128)S(1)} %get-tuple-element.28, f32[512,1]{0,1:T(1,128)S(1)} %convert_multiply_fusion.2), kind=kOutput, calls=%fused_computation.39 | convolution fusion | flops 25986048 | bytes 346624 | tf_op jit(solution)/shard_map/dot_general | solution.py:30
  12.6 1.2 %convolution_sine_fusion = f32[512,128]{1,0:T(8,128)S(1)} fusion(f32[512,128]{1,0:T(8,128)S(1)} %convolution_sine_fusion.1, f32[128,128]{1,0:T(8,128)S(1)} %copy-done.6), kind=kOutput, calls=%fused_computation.38 | convolution fusion | flops 100663296 | bytes 589824 | tf_op jit(solution)/shard_map/dot_general | solution.py:31
  13.7 0.8 %dynamic-slice_negate_fusion = f32[256]{0:T(256)S(1)} fusion(f32[1024]{0:T(1024)} %param.23, s32[]{:T(128)S(6)} %select_n.68), kind=kLoop, calls=%fused_computation.163 | loop fusion | flops 256 | bytes 2052 | tf_op jit(solution)/shard_map/neg | solution.py:37
  14.5 0.6 fusion.51
  15.1 0.1 multiply_exponential_fusion
  15.3 0.3 slice_multiply_fusion.3
  15.6 0.8 %reverse = f32[256,512]{1,0:T(8,128)S(1)} reverse(f32[256,512]{1,0:T(8,128)S(1)} %bitcast.119), dimensions={1} | reverse | bytes 1048576
  16.4 0.2 slice.175
  16.6 1.6 %convolution_multiply_fusion = f32[256,512]{1,0:T(8,128)S(1)} fusion(f32[512,128]{1,0:T(8,128)S(1)} %convolution_sine_fusion, f32[512]{0:T(512)S(1)} %convert_multiply_fusion, f32[256]{0:T(256)S(1)} %dynamic-slice_negate_fusion, f32[128,1024]{1,0:T(8,128)} %param.21, s32[]{:T(128)S(6)} %select_n.68), kind=kOutput, calls=%fused_computation.37 | convolution fusion | flops 201588736 | bytes 920580 | tf_op jit(solution)/shard_map/pf,fh->hp/dot_general | solution.py:36
  18.2 0.3 multiply_reduce_fusion
  18.5 0.3 copy.28
  18.8 0.1 fusion.36
  18.9 1.8 %convolution_bitcast_fusion = f32[256,128,2,8]{1,0,2,3:T(8,128)S(1)} fusion(f32[256,128,8,1]{0,2,1,3:T(8,128)S(1)} %fusion.36, f32[1,128,128]{1,2,0:T(8,128)S(1)} %get-tuple-element.32, f32[1,128,128]{1,2,0:T(8,128)S(1)} %get-tuple-element.33), kind=kOutput, calls=%fused_computation.27 | convolution fusion | flops 805339136 | bytes 3276800 | tf_op jit(solution)/shard_map/sfa,cab->cfsb/dot_general | solution.py:56
  20.8 1.2 %copy.62 = f32[256,128,2,8]{1,3,2,0:T(8,128)S(1)} copy(f32[256,128,2,8]{1,0,2,3:T(8,128)S(1)} %convolution_bitcast_fusion) | data formatting | bytes 4194304 | tf_op jit(solution)/shard_map/sfa,cab->cfsb/transpose | solution.py:56
  22.0 0.0 copy-start.3
  22.0 0.0 copy-start.11
  22.0 0.0 copy-start.12
  22.0 0.0 copy-start.13
  22.0 1.5 %fusion.118 = (f32[256,128,8]{1,2,0:T(8,128)}, f32[256,128,8]{1,2,0:T(8,128)}) fusion(f32[256,128,16]{1,2,0:T(8,128)S(1)} %bitcast.117), kind=kLoop, calls=%fused_computation.180 | loop fusion | bytes 4194304 | tf_op jit(solution)/shard_map/slice | solution.py:51
  23.5 0.0 copy-done.3
  23.5 0.7 %cosine_bitcast_fusion = (f32[64,1,128]{2,0,1:T(8,128)}, f32[64,1,128]{2,0,1:T(8,128)}) fusion(f32[128,128]{1,0:T(8,128)S(1)} %copy-done.3), kind=kLoop, calls=%fused_computation.110 | loop fusion | flops 8192 | bytes 98304 | tf_op jit(solution)/shard_map/stack | solution.py:133
  24.3 0.0 copy-done.12
  24.3 0.6 pad_maximum_fusion.14
  24.9 0.0 collective-permute-done
  25.0 0.0 collective-permute-done.1
  25.0 1.0 %maximum_convert_fusion = f32[3,130,1024]{2,1,0:T(8,128)S(1)} fusion(bf16[3,1,1024]{2,1,0:T(2,128)(2,1)} %collective-permute-done.1, bf16[3,128,1024]{2,1,0:T(8,128)(2,1)S(1)} %constant_dynamic-update-slice_fusion, bf16[3,1,1024]{2,1,0:T(2,128)(2,1)} %collective-permute-done), kind=kLoop, calls=%fused_computation.53 | loop fusion | flops 2396160 | bytes 2396160 | tf_op jit(solution)/shard_map/convert_element_type | solution.py:94
  25.9 0.5 fusion.24
  26.4 1.1 %copy-done.2 = f32[3,128,1024]{2,1,0:T(8,128)} copy-done((f32[3,128,1024]{2,1,0:T(8,128)}, f32[3,128,1024]{2,1,0:T(8,128)S(1)}, u32[]{:S(2)}) %copy-start.2) | copy-done | bytes 1572888
  27.6 0.1 fusion.48
  27.7 0.8 %pad_maximum_fusion.1 = f32[4,256,128]{1,2,0:T(8,128)} fusion(f32[1,256,128]{1,2,0:T(8,128)S(1)} %get-tuple-element.18, f32[1,256,128]{1,2,0:T(8,128)S(1)} %get-tuple-element.19, f32[1,256,128]{1,2,0:T(8,128)S(1)} %get-tuple-element.20, f32[1,256,128]{1,2,0:T(8,128)S(1)} %get-tuple-element.17), kind=kLoop, calls=%fused_computation.59 | loop fusion | flops 393216 | bytes 1048576 | tf_op jit(solution)/shard_map/stack | solution.py:102
  28.5 5.6 %all-to-all-start = ((f32[4,256,128]{1,2,0:T(8,128)}), f32[4,256,128]{1,2,0:T(8,128)S(1)}, u32[]{:S(2)}, u32[]{:S(2)}) async-start(f32[4,256,128]{1,2,0:T(8,128)} %pad_maximum_fusion.1), calls=%async_computation | async-start | bytes 1048576 | tf_op jit(solution)/shard_map/all_to_all | solution.py:102
  34.1 0.1 fusion.100
  34.1 6.1 %fusion.7 = f32[256,128,16]{1,2,0:T(8,128)} fusion(f32[256,128,8]{1,2,0:T(8,128)} %get-tuple-element.14, f32[256,128,8]{1,2,0:T(8,128)} %get-tuple-element.13, f32[128,16]{0,1:T(8,128)S(1)} %get-tuple-element.27, f32[128,16]{0,1:T(8,128)S(1)} %pad_maximum_fusion.12, f32[8,8]{0,1:T(8,128)S(1)} %fusion.100, f32[8,8]{0,1:T(8,128)S(1)} %copy-done.7, ...), kind=kOutput, calls=%fused_computation.9 | convolution fusion | flops 102761216 | bytes 6308608 | tf_op jit(solution)/shard_map/cfk,kl->cfl/dot_general | solution.py:59
  40.2 2.7 %all-to-all-done = f32[4,256,128]{1,2,0:T(8,128)S(1)} async-done(((f32[4,256,128]{1,2,0:T(8,128)}), f32[4,256,128]{1,2,0:T(8,128)S(1)}, u32[]{:S(2)}, u32[]{:S(2)}) %all-to-all-start) | async-done | bytes 524320 | tf_op jit(solution)/shard_map/all_to_all | solution.py:102
  42.9 1.9 %convolution_bitcast_fusion.1 = f32[256,128,2,8]{1,0,2,3:T(8,128)S(1)} fusion(f32[256,64,8,1]{0,2,1,3:T(8,128)S(1)} %bitcast.123, f32[1,128,128]{1,2,0:T(8,128)S(1)} %get-tuple-element.33, f32[1,128,128]{1,2,0:T(8,128)S(1)} %get-tuple-element.32), kind=kOutput, calls=%fused_computation.28 | convolution fusion | flops 402669568 | bytes 2752512 | tf_op jit(solution)/shard_map/sfa,cab->cfsb/dot_general | solution.py:56
  44.8 1.2 %copy.63 = f32[256,128,2,8]{1,3,2,0:T(8,128)S(1)} copy(f32[256,128,2,8]{1,0,2,3:T(8,128)S(1)} %convolution_bitcast_fusion.1) | data formatting | bytes 4194304 | tf_op jit(solution)/shard_map/sfa,cab->cfsb/transpose | solution.py:56
  46.0 0.1 fusion.117
  46.1 3.2 %fusion.2 = f32[256,128,16]{1,2,0:T(8,128)S(1)} fusion(f32[256,128,8]{1,2,0:T(8,128)S(1)} %get-tuple-element.12, f32[256,128,8]{1,2,0:T(8,128)S(1)} %get-tuple-element.11, f32[128,16]{0,1:T(8,128)S(1)} %get-tuple-element.27, f32[128,16]{0,1:T(8,128)S(1)} %pad_maximum_fusion.12, f32[8,8]{0,1:T(8,128)S(1)} %fusion.100, f32[8,8]{0,1:T(8,128)S(1)} %copy-done.7, ...), kind=kOutput, calls=%fused_computation.4 | convolution fusion | flops 102761216 | bytes 6308608 | tf_op jit(solution)/shard_map/cfk,kl->cfl/dot_general | solution.py:59
  49.3 0.2 multiply_subtract_fusion
  49.6 1.9 %fusion.11 = f32[256,128,16]{1,2,0:T(8,128)S(1)} fusion(f32[256,128,8]{1,2,0:T(8,128)S(1)} %get-tuple-element.8, f32[256,128,8]{1,2,0:T(8,128)S(1)} %get-tuple-element.7, f32[8,8]{0,1:T(8,128)S(1)} %fusion.100, f32[8,8]{0,1:T(8,128)S(1)} %copy-done.8, f32[8,8]{0,1:T(8,128)S(1)} %copy-done.7), kind=kOutput, calls=%fused_computation.12 | convolution fusion | flops 101188352 | bytes 4195072 | tf_op jit(solution)/shard_map/cfk,kl->cfl/dot_general | solution.py:65
  51.5 0.0 copy-start.4
  51.5 0.0 copy-start.5
  51.5 0.4 fusion.116
  51.9 0.4 copy-done.4
  52.2 0.0 copy-done.5
  52.3 1.8 %fusion.32 = f32[256,64,8]{1,2,0:T(8,128)S(1)} fusion(f32[256,128,8]{1,2,0:T(8,128)S(1)} %get-tuple-element.10, f32[256,128,8]{1,2,0:T(8,128)S(1)} %get-tuple-element.9, f32[256,128,16]{1,2,0:T(8,128)S(1)} %fusion.11, f32[128,16]{0,1:T(8,128)S(1)} %copy-done.9, f32[128,16]{0,1:T(8,128)S(1)} %pad_maximum_fusion.12, f32[64,1,128]{2,0,1:T(8,128)S(1)} %copy-done.5, ...), kind=kOutput, calls=%fused_computation.36 | convolution fusion | flops 404897792 | bytes 4800512 | tf_op jit(solution)/shard_map/asf,cfsb->cab/dot_general | solution.py:68
  54.1 0.0 copy-start.14
  54.1 0.4 copy.32
  54.5 11.2 %all_to_all.24 = f32[256,4,128]{0,2,1:T(8,128)S(1)} all-to-all(f32[256,4,128]{0,2,1:T(8,128)S(1)} %bitcast.121), channel_id=1, replica_groups=mesh['grp'=2,'row'=4,'col'=4] {'col'}, dimensions={1} | all-to-all | bytes 1048576 | tf_op jit(solution)/shard_map/all_to_all | solution.py:176
  65.8 4.3 %fusion = bf16[1,128,2048]{2,1,0:T(8,128)(2,1)} fusion(bf16[1024,2048]{1,0:T(8,128)(2,1)} %param.25, f32[3,128,1024]{2,1,0:T(8,128)} %copy-done.2, f32[1024,128]{0,1:T(8,128)S(1)} %bitcast.120, f32[1024]{0:T(1024)S(1)} %copy-done.14), kind=kOutput, calls=%fused_computation.1 | convolution fusion | flops 537788416 | bytes 6819840 | tf_op jit(solution)/shard_map/dot_general | solution.py:178
  (29 shorter events, 0.2 us)
Async XLA Ops:
  0.0 14.5 %copy-start = (f32[128,1024]{1,0:T(8,128)S(1)}, f32[128,1024]{1,0:T(8,128)}, u32[]{:S(2)}) copy-start(f32[128,1024]{1,0:T(8,128)} %param.22) | copy-start | bytes 1572868
  0.0 12.6 %copy-start.6 = (f32[128,128]{1,0:T(8,128)S(1)}, f32[128,128]{1,0:T(8,128)}, u32[]{:S(2)}) copy-start(f32[128,128]{1,0:T(8,128)} %param.20) | copy-start | bytes 196612
  3.6 21.3 %collective-permute-start = (bf16[3,1,1024]{2,1,0:T(2,128)(2,1)}, bf16[3,1,1024]{2,1,0:T(2,128)(2,1)}, u32[]{:S(2)}, u32[]{:S(2)}) collective-permute-start(bf16[3,1,1024]{2,1,0:T(2,128)(2,1)} %get-tuple-element.15), channel_id=1, source_target_pairs={{0,1},{1,2},{2,3},{4,5},{5,6},{6,7},{8,9},{9,10},{10,11},{12,13},{... | collective-permute-start | bytes 18440 | tf_op jit(solution)/shard_map/ppermute | solution.py:17
  6.6 18.4 %collective-permute-start.1 = (bf16[3,1,1024]{2,1,0:T(2,128)(2,1)}, bf16[3,1,1024]{2,1,0:T(2,128)(2,1)}, u32[]{:S(2)}, u32[]{:S(2)}) collective-permute-start(bf16[3,1,1024]{2,1,0:T(2,128)(2,1)} %get-tuple-element.16), channel_id=1, source_target_pairs={{1,0},{2,1},{3,2},{5,4},{6,5},{7,6},{9,8},{10,9},{11,10},{13,12},{... | collective-permute-start | bytes 18440 | tf_op jit(solution)/shard_map/ppermute | solution.py:18
  22.0 1.5 %copy-start.3 = (f32[128,128]{1,0:T(8,128)S(1)}, f32[128,128]{1,0:T(8,128)}, u32[]{:S(2)}) copy-start(f32[128,128]{1,0:T(8,128)} %fusion.64) | copy-start | bytes 196612
  22.0 2.3 %copy-start.11 = (f32[3,1024]{1,0:T(4,128)S(1)}, f32[3,1024]{1,0:T(4,128)}, u32[]{:S(2)}) copy-start(f32[3,1024]{1,0:T(4,128)} %param.18) | copy-start | bytes 36868
  22.0 2.3 %copy-start.12 = (f32[3,1024]{1,0:T(4,128)S(1)}, f32[3,1024]{1,0:T(4,128)}, u32[]{:S(2)}) copy-start(f32[3,1024]{1,0:T(4,128)} %param.17) | copy-start | bytes 36868
  22.0 2.2 %copy-start.13 = (f32[3,1024]{1,0:T(4,128)S(1)}, f32[3,1024]{1,0:T(4,128)}, u32[]{:S(2)}) copy-start(f32[3,1024]{1,0:T(4,128)} %param.16) | copy-start | bytes 36868
  22.0 2.9 %copy-start.10 = (f32[128,8]{0,1:T(8,128)S(1)}, f32[128,8]{0,1:T(8,128)}, u32[]{:S(2)}) copy-start(f32[128,8]{0,1:T(8,128)} %fusion.102) | copy-start | bytes 12292
  26.4 1.1 %copy-start.2 = (f32[3,128,1024]{2,1,0:T(8,128)}, f32[3,128,1024]{2,1,0:T(8,128)S(1)}, u32[]{:S(2)}) copy-start(f32[3,128,1024]{2,1,0:T(8,128)S(1)} %fusion.24) | copy-start | bytes 4718596
  27.6 6.6 %copy-start.7 = (f32[8,8]{0,1:T(8,128)S(1)}, f32[8,8]{0,1:T(8,128)}, u32[]{:S(2)}) copy-start(f32[8,8]{0,1:T(8,128)} %get-tuple-element.36) | copy-start | bytes 772
  27.6 6.6 %copy-start.8 = (f32[8,8]{0,1:T(8,128)S(1)}, f32[8,8]{0,1:T(8,128)}, u32[]{:S(2)}) copy-start(f32[8,8]{0,1:T(8,128)} %get-tuple-element.37) | copy-start | bytes 772
  28.5 14.4 %all-to-all-start = ((f32[4,256,128]{1,2,0:T(8,128)}), f32[4,256,128]{1,2,0:T(8,128)S(1)}, u32[]{:S(2)}, u32[]{:S(2)}) async-start(f32[4,256,128]{1,2,0:T(8,128)} %pad_maximum_fusion.1), calls=%async_computation | async-start | bytes 1048576 | tf_op jit(solution)/shard_map/all_to_all | solution.py:102
  46.1 3.2 %copy-start.1 = (f32[256,128,16]{1,2,0:T(8,128)S(1)}, f32[256,128,16]{1,2,0:T(8,128)}, u32[]{:S(2)}) copy-start(f32[256,128,16]{1,2,0:T(8,128)} %fusion.7) | copy-start | bytes 6291460
  51.5 0.8 %copy-start.4 = (f32[64,1,128]{2,0,1:T(8,128)S(1)}, f32[64,1,128]{2,0,1:T(8,128)}, u32[]{:S(2)}) copy-start(f32[64,1,128]{2,0,1:T(8,128)} %get-tuple-element.21) | copy-start | bytes 98308
  51.5 0.8 %copy-start.5 = (f32[64,1,128]{2,0,1:T(8,128)S(1)}, f32[64,1,128]{2,0,1:T(8,128)}, u32[]{:S(2)}) copy-start(f32[64,1,128]{2,0,1:T(8,128)} %get-tuple-element.22) | copy-start | bytes 98308
  51.5 0.8 %copy-start.9 = (f32[128,16]{0,1:T(8,128)S(1)}, f32[128,16]{0,1:T(8,128)}, u32[]{:S(2)}) copy-start(f32[128,16]{0,1:T(8,128)} %get-tuple-element.26) | copy-start | bytes 24580
  54.1 11.7 %copy-start.14 = (f32[1024]{0:T(1024)S(1)}, f32[1024]{0:T(1024)}, u32[]{:S(2)}) copy-start(f32[1024]{0:T(1024)} %param.24) | copy-start | bytes 12292
